TPU v7x, 32 devices: a whole 2x2x4 slice. The times are simulated.
32 devices in a mesh: ep: 32 (over z, y, x, core).
Axes of the slice: x: 2, y: 2, z: 4, core: 2. Of those that a mesh axis runs over, the one named last changes fastest.
Arguments:
- tokens: bfloat16 [384, 2048], P('ep'), may hold values from -6 to 6
- cache_latent: bfloat16 [384, 1024, 512], P('ep'), may hold values from -180 to 180
- cache_rope: bfloat16 [384, 1024, 64], P('ep'), may hold values from -6 to 6
- cache_lengths: int32 [384], P('ep'), may hold values from 1 to 1024, as said below
- expert_ids: int32 [384, 6], P('ep'), may hold values from 0 to 15, as said below
- route_weight: float32 [384, 6], P('ep'), may hold values from 1 to 2
- attn_gain: float32 [2048], replicated, may hold values from 0.1 to 1.9
- q_gain: float32 [512], replicated, may hold values from 0.1 to 1.9
- kv_gain: float32 [512], replicated, may hold values from 0.1 to 1.9
- moe_gain: float32 [2048], replicated, may hold values from 0.1 to 1.9
- w_qdown: bfloat16 [2048, 512], replicated, may hold values from -0.125 to 0.125
- w_kvdown: bfloat16 [2048, 512], replicated, may hold values from -0.125 to 0.125
- w_krope: bfloat16 [2048, 64], replicated, may hold values from -0.125 to 0.125
- w_qup: bfloat16 [512, 1536], replicated, may hold values from -0.25 to 0.25
- w_kup: bfloat16 [512, 1024], replicated, may hold values from -0.5 to 0.5
- w_vup: bfloat16 [512, 1024], replicated, may hold values from -0.25 to 0.25
- w_out: bfloat16 [1024, 2048], replicated, may hold values from -0.1875 to 0.1875
- expert_gate: bfloat16 [32, 2048, 256], P('ep'), may hold values from -0.125 to 0.125
- expert_up: bfloat16 [32, 2048, 256], P('ep'), may hold values from -0.125 to 0.125
- expert_down: bfloat16 [32, 256, 2048], P('ep'), may hold values from -0.25 to 0.25
Outputs:
- mixed: float32 [384, 2048], P('ep')
- new_latent: bfloat16 [384, 512], P('ep')
- new_rope_key: bfloat16 [384, 64], P('ep')
Inputs may be any that keep to these rules, and one draw needn't show every extreme that they name: `cache_lengths`: some sequence holds 1024 positions. `expert_ids`: each row names 6 different experts of one group g, numbered g * 16 to g * 16 + 15; among the rows of one device no expert is named more than 5 times, and some expert exactly 5 times.
All inputs are finite; a program needn't handle non-finite values.
Results may differ from a plain program's by a relative error of at most 0.03.
Values may be sent and summed in bfloat16 or wider, within the bound.
A program may use at most 128 MiB of HBM per device.

v0:
```python
import jax
import jax.numpy as jnp
from jax import lax
from jax.sharding import PartitionSpec as P

HEADS = 8
KV_RANK = 512
NOPE_DIM = 128
ROPE_DIM = 64
VALUE_DIM = 128
GROUP_SIZE = 16
TOP_K = 6
BLOCK_POS = 512
SEQ_DEV = 12


EPS = 1e-06
THETA = 10000.0


def partner(value, axis, bit):
    mask = 2**bit
    pairs = [(source, source ^ mask) for source in range(lax.axis_size(axis))]
    return lax.ppermute(value, axis, pairs)


def norm_gain(values, gain_vec):
    values = values.astype(jnp.float32)
    return values * lax.rsqrt(jnp.mean(values * values, axis=-1, keepdims=True) + EPS) * gain_vec


def rotary_angles(lengths):
    half_width = ROPE_DIM // 2
    inverse = THETA ** (-jnp.arange(half_width, dtype=jnp.float32) / half_width)
    return lengths.astype(jnp.float32)[:, None] * inverse[None, :]


def rotate(values, angles):
    half_width = values.shape[-1] // 2
    first_half = values[..., :half_width]
    second = values[..., half_width:]
    cosine = jnp.cos(angles)
    sine_part = jnp.sin(angles)
    return jnp.concatenate(
        [first_half * cosine - second * sine_part, second * cosine + first_half * sine_part],
        axis=-1,
    )


def attend(
    tokens,
    cache_latent,
    cache_rope,
    cache_lengths,
    attn_gain,
    q_gain,
    kv_gain,
    w_qdown,
    w_kvdown,
    w_krope,
    w_qup,
    w_kup,
    w_vup,
    w_out,
):
    row_count = tokens.shape[0]
    score_scale = (NOPE_DIM + ROPE_DIM) ** (-0.5)
    normed = norm_gain(tokens, attn_gain).astype(jnp.bfloat16)
    q_low = norm_gain(jnp.dot(normed, w_qdown, preferred_element_type=jnp.float32), q_gain).astype(
        jnp.bfloat16
    )
    query_all = jnp.dot(q_low, w_qup, preferred_element_type=jnp.float32).reshape(
        row_count, HEADS, NOPE_DIM + ROPE_DIM
    )
    angles = rotary_angles(cache_lengths)
    q_nope = query_all[:, :, :NOPE_DIM].astype(jnp.bfloat16)
    q_rope = rotate(query_all[:, :, NOPE_DIM:], angles[:, None, :]).astype(jnp.bfloat16)
    new_latent = norm_gain(
        jnp.dot(normed, w_kvdown, preferred_element_type=jnp.float32), kv_gain
    ).astype(jnp.bfloat16)
    new_rope_key = rotate(
        jnp.dot(normed, w_krope, preferred_element_type=jnp.float32), angles
    ).astype(jnp.bfloat16)
    q_latent = jnp.einsum(
        "thn,chn->thc",
        q_nope,
        w_kup.reshape(KV_RANK, HEADS, NOPE_DIM),
        preferred_element_type=jnp.float32,
    ).astype(jnp.bfloat16)
    own_score = (
        jnp.einsum("thc,tc->th", q_latent, new_latent, preferred_element_type=jnp.float32)
        + jnp.einsum("thr,tr->th", q_rope, new_rope_key, preferred_element_type=jnp.float32)
    ) * score_scale
    run_sum = jnp.broadcast_to(
        new_latent.astype(jnp.float32)[:, None, :], (row_count, HEADS, KV_RANK)
    )
    run_total = jnp.ones((row_count, HEADS), jnp.float32)
    block_total = (jnp.max(cache_lengths) + BLOCK_POS - 1) // BLOCK_POS

    def block_step(block_index, carry):
        run_peak, run_total, run_sum = carry
        block_start = block_index * BLOCK_POS
        latent_block = lax.dynamic_slice_in_dim(cache_latent, block_start, BLOCK_POS, 1)
        rope_block = lax.dynamic_slice_in_dim(cache_rope, block_start, BLOCK_POS, 1)
        scores = (
            jnp.einsum("thc,tpc->thp", q_latent, latent_block, preferred_element_type=jnp.float32)
            + jnp.einsum("thr,tpr->thp", q_rope, rope_block, preferred_element_type=jnp.float32)
        ) * score_scale
        valid_mask = (block_start + jnp.arange(BLOCK_POS, dtype=jnp.int32))[
            None, None, :
        ] < cache_lengths[:, None, None]
        scores = jnp.where(valid_mask, scores, -jnp.inf)
        new_peak = jnp.maximum(run_peak, jnp.max(scores, axis=2))
        shrink = jnp.exp(run_peak - new_peak)
        block_probs = jnp.exp(scores - new_peak[:, :, None])
        run_total = run_total * shrink + jnp.sum(block_probs, axis=2)
        run_sum = run_sum * shrink[:, :, None] + jnp.einsum(
            "thp,tpc->thc",
            block_probs.astype(jnp.bfloat16),
            latent_block,
            preferred_element_type=jnp.float32,
        )
        return (new_peak, run_total, run_sum)

    run_peak, run_total, run_sum = lax.fori_loop(
        0, block_total, block_step, (own_score, run_total, run_sum)
    )
    o_latent = (run_sum / run_total[:, :, None]).astype(jnp.bfloat16)
    heads_out = (
        jnp.einsum(
            "thc,chv->thv",
            o_latent,
            w_vup.reshape(KV_RANK, HEADS, VALUE_DIM),
            preferred_element_type=jnp.float32,
        )
        .astype(jnp.bfloat16)
        .reshape(row_count, HEADS * VALUE_DIM)
    )
    mixed_attn = (
        tokens.astype(jnp.float32) + jnp.dot(heads_out, w_out, preferred_element_type=jnp.float32)
    ).astype(jnp.bfloat16)
    return (mixed_attn, new_latent, new_rope_key)


def capacity_of(half_count):
    group_count = half_count // 2 // GROUP_SIZE
    group_most = min(SEQ_DEV, max(3, 2 * ((SEQ_DEV + group_count - 1) // group_count)))
    return (TOP_K * group_most + GROUP_SIZE - 1) // GROUP_SIZE


def mix_experts(moe_in, expert_ids, route_weight, expert_gate, expert_up, expert_down):
    row_count, model_width = moe_in.shape
    top_count = expert_ids.shape[1]
    half_count = lax.axis_size("ep")
    slot_count = capacity_of(half_count)
    per_core = (slot_count + 1) // 2
    gate_half = expert_gate[0]
    up_half = expert_up[0]
    down_half = expert_down[0]
    flat_ids = expert_ids.reshape(-1)
    one_hot = (flat_ids[:, None] == jnp.arange(half_count // 2, dtype=jnp.int32)[None, :]).astype(
        jnp.int32
    )
    earlier = jnp.cumsum(one_hot, axis=0) - one_hot
    slot_rank = jnp.sum(earlier * one_hot, axis=1)
    owner_ids = jnp.arange(half_count, dtype=jnp.int32) // 2
    parity_ids = jnp.arange(half_count, dtype=jnp.int32) % 2
    wanted_rank = (
        2 * jnp.arange(per_core, dtype=jnp.int32)[None, None, :] + parity_ids[None, :, None]
    )
    placed = (flat_ids[:, None, None] == owner_ids[None, :, None]) & (
        slot_rank[:, None, None] == wanted_rank
    )
    placed = placed.reshape(row_count * top_count, half_count * per_core).astype(jnp.float32)
    chosen = jnp.max(placed.reshape(row_count, top_count, half_count * per_core), axis=1).astype(
        jnp.bfloat16
    )
    outgoing = jnp.einsum("sx,sd->xd", chosen, moe_in, preferred_element_type=jnp.float32).astype(
        jnp.bfloat16
    )
    own_rows = lax.all_to_all(
        outgoing.reshape(half_count, per_core, model_width),
        "ep",
        split_axis=0,
        concat_axis=0,
        tiled=True,
    )
    sibling = partner(own_rows, "ep", 0)
    slot_rows = jnp.concatenate([own_rows, sibling], axis=1)
    flat_rows = slot_rows.reshape(-1, model_width)
    hidden = (
        jax.nn.silu(jnp.dot(flat_rows, gate_half, preferred_element_type=jnp.float32))
        * jnp.dot(flat_rows, up_half, preferred_element_type=jnp.float32)
    ).astype(jnp.bfloat16)
    outputs = (
        jnp.dot(hidden, down_half, preferred_element_type=jnp.float32)
        .astype(jnp.bfloat16)
        .reshape(slot_rows.shape)
    )
    from_sibling = partner(outputs[:, per_core:], "ep", 0)
    pair_sum = outputs[:, :per_core].astype(jnp.float32) + from_sibling.astype(jnp.float32)
    returned = lax.all_to_all(pair_sum, "ep", split_axis=0, concat_axis=0, tiled=True)
    per_route = jnp.dot(
        placed,
        returned.reshape(half_count * per_core, model_width),
        precision=lax.Precision.HIGHEST,
        preferred_element_type=jnp.float32,
    )
    per_route = per_route.reshape(row_count, top_count, model_width)
    return jnp.sum(route_weight[:, :, None] * per_route, axis=1)


def shards(
    tokens,
    cache_latent,
    cache_rope,
    cache_lengths,
    expert_ids,
    route_weight,
    attn_gain,
    q_gain,
    kv_gain,
    moe_gain,
    w_qdown,
    w_kvdown,
    w_krope,
    w_qup,
    w_kup,
    w_vup,
    w_out,
    expert_gate,
    expert_up,
    expert_down,
):
    mixer_weights = (
        attn_gain,
        q_gain,
        kv_gain,
        w_qdown,
        w_kvdown,
        w_krope,
        w_qup,
        w_kup,
        w_vup,
        w_out,
    )
    mixed_attn, new_latent, new_rope_key = attend(
        tokens, cache_latent, cache_rope, cache_lengths, *mixer_weights
    )
    moe_in = norm_gain(mixed_attn, moe_gain).astype(jnp.bfloat16)
    moe_out = mix_experts(moe_in, expert_ids, route_weight, expert_gate, expert_up, expert_down)
    mixed = mixed_attn.astype(jnp.float32) + moe_out
    return (mixed, new_latent, new_rope_key)


def solution(mesh):
    placed = (
        P("ep", None),
        P("ep", None, None),
        P("ep", None, None),
        P("ep"),
        P("ep", None),
        P("ep", None),
        P(),
        P(),
        P(),
        P(),
        P(),
        P(),
        P(),
        P(),
        P(),
        P(),
        P(),
        P("ep", None, None),
        P("ep", None, None),
        P("ep", None, None),
    )
    return jax.shard_map(
        shards,
        mesh=mesh,
        in_specs=placed,
        out_specs=(P("ep", None), P("ep", None), P("ep", None)),
        check_vma=False,
    )
```

profile of v0, /device:TPU:0, one launch (start us, length us, event | category | flops | bytes accessed | tf_op | source)
XLA Modules:
  0.0 108.4 jit_solution(619388758719337516)
XLA Ops:
  0.7 1.5 %fusion.63 = (s32[]{:T(128)}, f32[12]{0:T(128)S(1)}) fusion(s32[12]{0:T(128)} %param.25), kind=kLoop, calls=%fused_computation.104 | loop fusion | flops 23 | bytes 100 | tf_op jit(solution)/shard_map/reduce_max | solution.py:98
  2.8 0.5 multiply_power_fusion
  3.3 1.0 fusion.33
  4.3 1.4 %multiply_reduce_fusion.1 = (f32[12]{0:T(128)S(1)}, f32[12,512]{1,0:T(8,128)S(1)}) fusion(bf16[2048,512]{1,0:T(8,128)(2,1)S(1)} %copy-done, bf16[12,2048]{1,0:T(8,128)(2,1)} %param.22, f32[2048]{0:T(1024)} %param.28, f32[12]{0:T(128)S(1)} %add_rsqrt_fusion.3), kind=kOutput, calls=%fused_computation.67 | convolution fusion | flops 25276404 | bytes 2179168 | tf_op jit(solution)/shard_map/dot_general | solution.py:79
  5.9 0.6 and_select_fusion.1
  6.5 2.3 %multiply_reduce_fusion.2 = (f32[12]{0:T(128)S(1)}, f32[12,512]{1,0:T(8,128)S(1)}) fusion(bf16[2048,512]{1,0:T(8,128)(2,1)} %param.32, bf16[12,2048]{1,0:T(8,128)(2,1)S(1)} %copy-done.3, f32[2048]{0:T(1024)S(1)} %copy-done.6, f32[12]{0:T(128)S(1)} %add_rsqrt_fusion.3), kind=kOutput, calls=%fused_computation.69 | convolution fusion | flops 25276404 | bytes 2179168 | tf_op jit(solution)/shard_map/dot_general | solution.py:69
  8.8 0.4 fusion.49
  9.2 0.1 reshape.305
  9.3 1.2 %fusion.56 = f32[12,64]{1,0:T(8,128)S(1)} fusion(bf16[2048,64]{0,1:T(8,128)(2,1)} %param.34, bf16[12,2048]{1,0:T(8,128)(2,1)S(1)} %copy-done.3, f32[2048]{0:T(1024)S(1)} %copy-done.6, f32[12]{0:T(128)S(1)} %add_rsqrt_fusion.3), kind=kOutput, calls=%fused_computation.100 | convolution fusion | flops 3244032 | bytes 322608 | tf_op jit(solution)/shard_map/dot_general | solution.py:82
  10.5 0.4 fusion.21
  10.9 0.1 copy.50
  11.0 0.8 subtract_convert_fusion.1
  11.7 0.1 subtract_convert_fusion
  11.8 0.1 pad_maximum_fusion.1
  11.9 0.1 fusion.79
  12.0 0.1 fusion.53
  12.1 0.1 fusion.46
  12.3 18.1 %while.14 = (s32[]{:T(128)}, f32[12,8]{1,0:T(8,128)S(1)}, f32[12,8]{1,0:T(8,128)S(1)}, f32[12,8,512]{2,1,0:T(8,128)S(1)}, s32[]{:T(128)}, /*index=5*/s32[12]{0:T...) while((s32[]{:T(128)}, f32[12,8]{1,0:T(8,128)S(1)}, ...), condition=%wide.region_7.8_spmd, body=%wide.region_4.7_spmd.sunk | while | flops 107453120 | bytes 21184784 | solution.py:125
  12.4 4.6 %fusion.96 = f32[12,512,8]{1,2,0:T(8,128)S(1)} fusion(bf16[12,8,512]{2,1,0:T(8,128)(2,1)S(1)} %get-tuple-element.242, bf16[12,1024,512]{2,1,0:T(8,128)(2,1)} %get-tuple-element.241, s32[]{:T(128)S(6)} %select_n.46), kind=kOutput, calls=%fused_computation.2.clone.1 | convolution fusion | flops 50331648 | bytes 6586372 | tf_op jit(solution)/shard_map/while/body/thc,tpc->thp/dot_general | solution.py:106
  17.0 0.1 broadcast_compare_fusion.3
  17.1 0.3 fusion.97
  17.4 0.2 fusion.98
  17.6 3.7 %fusion.99 = f32[12,8,512]{2,1,0:T(8,128)S(1)} fusion(bf16[12,1024,512]{2,1,0:T(8,128)(2,1)} %get-tuple-element.241, s32[]{:T(128)S(6)} %select_n.46, f32[12,8,512]{2,1,0:T(8,128)S(1)} %get-tuple-element.224, f32[12,8,512]{2,1,0:T(8,128)S(1)} %get-tuple-element.204, f32[12,8]{1,0:T(8,128)S(1)} %get-tuple-element.206, f32[12,8]{1,0:T(8,128)S(1)} %max.4), kind=kOutput, calls=%fused_computation.6.clone.1 | convolution fusion | flops 50528256 | bytes 6882052 | tf_op jit(solution)/shard_map/while/body/thp,tpc->thc/dot_general | solution.py:117
  21.4 4.6 %fusion.96 = f32[12,512,8]{1,2,0:T(8,128)S(1)} fusion(bf16[12,8,512]{2,1,0:T(8,128)(2,1)S(1)} %get-tuple-element.242, bf16[12,1024,512]{2,1,0:T(8,128)(2,1)} %get-tuple-element.241, s32[]{:T(128)S(6)} %select_n.46), kind=kOutput, calls=%fused_computation.2.clone.1 | convolution fusion | flops 50331648 | bytes 6586372 | tf_op jit(solution)/shard_map/while/body/thc,tpc->thp/dot_general | solution.py:106
  26.0 0.1 broadcast_compare_fusion.3
  26.1 0.3 fusion.97
  26.4 0.2 fusion.98
  26.6 3.7 %fusion.99 = f32[12,8,512]{2,1,0:T(8,128)S(1)} fusion(bf16[12,1024,512]{2,1,0:T(8,128)(2,1)} %get-tuple-element.241, s32[]{:T(128)S(6)} %select_n.46, f32[12,8,512]{2,1,0:T(8,128)S(1)} %get-tuple-element.224, f32[12,8,512]{2,1,0:T(8,128)S(1)} %get-tuple-element.204, f32[12,8]{1,0:T(8,128)S(1)} %get-tuple-element.206, f32[12,8]{1,0:T(8,128)S(1)} %max.4), kind=kOutput, calls=%fused_computation.6.clone.1 | convolution fusion | flops 50528256 | bytes 6882052 | tf_op jit(solution)/shard_map/while/body/thp,tpc->thc/dot_general | solution.py:117
  30.4 0.1 divide_convert_fusion
  30.5 1.5 %fusion.22 = bf16[12,8,128]{2,0,1:T(8,128)(2,1)S(1)} fusion(bf16[12,8,512]{2,1,0:T(8,128)(2,1)S(1)} %divide_convert_fusion, bf16[512,1024]{1,0:T(8,128)(2,1)} %param.37), kind=kOutput, calls=%fused_computation.31 | convolution fusion | flops 12595200 | bytes 1171456 | tf_op jit(solution)/shard_map/thc,chv->thv/dot_general | solution.py:130
  32.1 3.0 %multiply_reduce_fusion = (f32[12]{0:T(128)S(1)}, f32[12,2048]{1,0:T(8,128)S(1)}) fusion(bf16[12,1024]{1,0:T(8,128)(2,1)S(1)} %bitcast.70, bf16[1024,2048]{1,0:T(8,128)(2,1)} %param.38, bf16[12,2048]{1,0:T(8,128)(2,1)S(1)} %copy-done.3), kind=kOutput, calls=%fused_computation.54 | convolution fusion | flops 50479092 | bytes 4366384 | tf_op jit(solution)/shard_map/dot_general | solution.py:140
  35.1 0.1 copy.55
  35.2 0.1 eq.66
  35.3 0.1 fusion.44
  35.4 0.1 reduce_window_sum.11
  35.5 0.2 select_reduce_fusion
  35.7 0.1 eq.76
  35.7 0.1 broadcast_compare_fusion.1
  35.9 0.4 and.62
  36.3 0.1 add.143
  36.4 0.1 add.145
  36.6 0.4 convert_reduce_fusion
  37.0 0.3 convolution_convert_fusion.1
  37.3 0.2 reshape.309
  37.5 22.7 %all_to_all.10 = bf16[32,3,2048]{2,1,0:T(4,128)(2,1)S(1)} all-to-all(bf16[32,3,2048]{2,1,0:T(4,128)(2,1)S(1)} %reshape.309), channel_id=1, replica_groups=mesh['ep'=32] {'ep'}, dimensions={0} | all-to-all | bytes 786432 | tf_op jit(solution)/shard_map/all_to_all | solution.py:181
  60.3 1.9 %collective-permute-done = bf16[32,3,2048]{2,1,0:T(4,128)(2,1)S(1)} collective-permute-done((bf16[32,3,2048]{2,1,0:T(4,128)(2,1)S(1)}, bf16[32,3,2048]{2,1,0:T(4,128)(2,1)S(1)}, u32[]{:S(2)}, u32[]{:S(2)}) %collective-permute-start) | collective-permute-done | bytes 393248 | tf_op jit(solution)/shard_map/ppermute | solution.py:24
  62.2 1.5 %pad_maximum_fusion = bf16[32,6,2048]{2,1,0:T(8,128)(2,1)} fusion(bf16[32,3,2048]{2,1,0:T(4,128)(2,1)S(1)} %collective-permute-done, bf16[32,3,2048]{2,1,0:T(4,128)(2,1)S(1)} %all_to_all.10), kind=kLoop, calls=%fused_computation.36 | loop fusion | flops 1572864 | bytes 1572864 | tf_op jit(solution)/shard_map/concatenate | solution.py:189
  63.7 1.4 %reshape.310 = bf16[192,2048]{1,0:T(8,128)(2,1)S(1)} reshape(bf16[32,6,2048]{2,1,0:T(8,128)(2,1)} %pad_maximum_fusion) | data formatting | bytes 1572864 | tf_op jit(solution)/shard_map/reshape | solution.py:190
  65.1 1.6 %fusion.28 = f32[192,256]{1,0:T(8,128)S(1)} fusion(bf16[192,2048]{1,0:T(8,128)(2,1)S(1)} %reshape.310, bf16[1,2048,256]{2,1,0:T(8,128)(2,1)} %param.40), kind=kOutput, calls=%fused_computation.38 | convolution fusion | flops 201326592 | bytes 2031616 | tf_op jit(solution)/shard_map/dot_general | solution.py:193
  66.7 3.5 %convolution_convert_fusion = bf16[192,2048]{1,0:T(8,128)(2,1)} fusion(bf16[1,256,2048]{2,1,0:T(8,128)(2,1)} %param.41, f32[192,256]{1,0:T(8,128)S(1)} %fusion.28, bf16[192,2048]{1,0:T(8,128)(2,1)S(1)} %reshape.310, bf16[1,2048,256]{2,1,0:T(8,128)(2,1)} %param.39), kind=kOutput, calls=%fused_computation.21 | convolution fusion | flops 403341312 | bytes 3866624 | tf_op jit(solution)/shard_map/dot_general | solution.py:196
  70.2 1.3 %reshape.311 = bf16[32,6,2048]{2,1,0:T(8,128)(2,1)S(1)} reshape(bf16[192,2048]{1,0:T(8,128)(2,1)} %convolution_convert_fusion) | data formatting | bytes 1572864 | tf_op jit(solution)/shard_map/reshape | solution.py:198
  71.5 0.3 slice.38
  71.9 0.2 collective-permute-start.1
  72.1 1.8 %collective-permute-done.1 = bf16[32,3,2048]{2,1,0:T(4,128)(2,1)S(1)} collective-permute-done((bf16[32,3,2048]{2,1,0:T(4,128)(2,1)S(1)}, bf16[32,3,2048]{2,1,0:T(4,128)(2,1)S(1)}, u32[]{:S(2)}, u32[]{:S(2)}) %collective-permute-start.1) | collective-permute-done | bytes 393248 | tf_op jit(solution)/shard_map/ppermute | solution.py:24
  73.8 1.3 %convert_add_fusion = f32[32,3,2048]{2,1,0:T(4,128)} fusion(bf16[32,3,2048]{2,1,0:T(4,128)(2,1)S(1)} %collective-permute-done.1, bf16[32,6,2048]{2,1,0:T(8,128)(2,1)S(1)} %reshape.311), kind=kLoop, calls=%fused_computation.42 | loop fusion | flops 589824 | bytes 1572864 | tf_op jit(solution)/shard_map/add | solution.py:201
  75.2 3.0 %all-to-all-start.1 = ((f32[32,3,2048]{2,1,0:T(4,128)}), f32[32,3,2048]{2,1,0:T(4,128)S(1)}, u32[]{:S(2)}, u32[]{:S(2)}) async-start(f32[32,3,2048]{2,1,0:T(4,128)} %convert_add_fusion), calls=%async_computation.1 | async-start | bytes 2097152 | tf_op jit(solution)/shard_map/all_to_all | solution.py:202
  78.2 0.1 compare_and_fusion
  78.3 0.4 and.61
  78.7 0.1 copy.54
  78.8 0.7 pad_maximum_fusion.2
  79.5 24.8 %all-to-all-done.1 = f32[32,3,2048]{2,1,0:T(4,128)S(1)} async-done(((f32[32,3,2048]{2,1,0:T(4,128)}), f32[32,3,2048]{2,1,0:T(4,128)S(1)}, u32[]{:S(2)}, u32[]{:S(2)}) %all-to-all-start.1) | async-done | bytes 786464 | tf_op jit(solution)/shard_map/all_to_all | solution.py:202
  104.4 1.3 %reshape.317 = f32[96,2048,1]{1,0,2:T(8,128)} reshape(f32[32,3,2048]{2,1,0:T(4,128)S(1)} %all-to-all-done.1) | data formatting | bytes 1572864 | tf_op jit(solution)/shard_map/reshape | solution.py:205
  105.6 2.1 %fusion.20 = f32[12,2048]{1,0:T(8,128)S(1)} fusion(f32[96,2048,1]{1,0,2:T(8,128)} %reshape.317, pred[12,6,96]{1,0,2:T(8,128)(4,1)S(1)} %and.61, f32[12,6]{1,0:T(8,128)S(1)} %copy.54), kind=kOutput, calls=%fused_computation.27 | convolution fusion | flops 170139648 | bytes 891936 | tf_op jit(solution)/shard_map/dot_general | solution.py:203
  107.7 0.7 add.150
  (59 shorter events, 0.6 us)
Async XLA Ops:
  0.6 3.7 %copy-start = (bf16[2048,512]{1,0:T(8,128)(2,1)S(1)}, bf16[2048,512]{1,0:T(8,128)(2,1)}, u32[]{:S(2)}) copy-start(bf16[2048,512]{1,0:T(8,128)(2,1)} %param.33) | copy-start | bytes 6291460
  0.6 5.8 %copy-start.3 = (bf16[12,2048]{1,0:T(8,128)(2,1)S(1)}, bf16[12,2048]{1,0:T(8,128)(2,1)}, u32[]{:S(2)}) copy-start(bf16[12,2048]{1,0:T(8,128)(2,1)} %param.22) | copy-start | bytes 147460
  0.7 5.8 %copy-start.6 = (f32[2048]{0:T(1024)S(1)}, f32[2048]{0:T(1024)}, u32[]{:S(2)}) copy-start(f32[2048]{0:T(1024)} %param.28) | copy-start | bytes 24580
  0.7 5.0 %copy-start.9 = (f32[512]{0:T(512)S(1)}, f32[512]{0:T(512)}, u32[]{:S(2)}) copy-start(f32[512]{0:T(512)} %param.30) | copy-start | bytes 6148
  4.3 4.5 %copy-start.12 = (f32[512]{0:T(512)S(1)}, f32[512]{0:T(512)}, u32[]{:S(2)}) copy-start(f32[512]{0:T(512)} %param.29) | copy-start | bytes 6148
  5.9 6.4 %copy-start.5 = (bf16[12,512]{1,0:T(8,128)(2,1)}, bf16[12,512]{1,0:T(8,128)(2,1)S(1)}, u32[]{:S(2)}) copy-start(bf16[12,512]{1,0:T(8,128)(2,1)S(1)} %multiply_convert_fusion.4) | copy-start | bytes 36868
  6.5 2.3 %copy-start.2 = (bf16[512,1536]{1,0:T(8,128)(2,1)S(1)}, bf16[512,1536]{1,0:T(8,128)(2,1)}, u32[]{:S(2)}) copy-start(bf16[512,1536]{1,0:T(8,128)(2,1)} %param.35) | copy-start | bytes 4718596
  6.5 4.0 %copy-start.4 = (bf16[512,1024]{1,0:T(8,128)(2,1)S(1)}, bf16[512,1024]{1,0:T(8,128)(2,1)}, u32[]{:S(2)}) copy-start(bf16[512,1024]{1,0:T(8,128)(2,1)} %param.36) | copy-start | bytes 3145732
  8.8 3.5 %copy-start.7 = (s32[12]{0:T(128)S(1)}, s32[12]{0:T(128)}, u32[]{:S(2)}) copy-start(s32[12]{0:T(128)} %param.25) | copy-start | bytes 148
  12.4 4.7 %copy-start.1 = (bf16[12,1024,64]{1,2,0:T(8,128)(2,1)S(1)}, bf16[12,1024,64]{1,2,0:T(8,128)(2,1)}, u32[]{:S(2)}) copy-start(bf16[12,1024,64]{1,2,0:T(8,128)(2,1)} %get-tuple-element.243) | copy-start | bytes 4718596 | tf_op jit(solution)/shard_map/while
  21.4 4.7 %copy-start.1 = (bf16[12,1024,64]{1,2,0:T(8,128)(2,1)S(1)}, bf16[12,1024,64]{1,2,0:T(8,128)(2,1)}, u32[]{:S(2)}) copy-start(bf16[12,1024,64]{1,2,0:T(8,128)(2,1)} %get-tuple-element.243) | copy-start | bytes 4718596 | tf_op jit(solution)/shard_map/while
  32.1 3.0 %copy-start.10 = (s32[12,6]{0,1:T(8,128)S(1)}, s32[12,6]{0,1:T(8,128)}, u32[]{:S(2)}) copy-start(s32[12,6]{0,1:T(8,128)} %param.26) | copy-start | bytes 868
  32.1 3.6 %copy-start.13 = (s32[32]{0:T(128)S(1)}, s32[32]{0:T(128)}, u32[]{:S(2)}) copy-start(s32[32]{0:T(128)} %and_select_fusion.1) | copy-start | bytes 388
  32.1 4.9 %copy-start.8 = (f32[2048]{0:T(1024)S(1)}, f32[2048]{0:T(1024)}, u32[]{:S(2)}) copy-start(f32[2048]{0:T(1024)} %param.31) | copy-start | bytes 24580
  60.3 1.9 %collective-permute-start = (bf16[32,3,2048]{2,1,0:T(4,128)(2,1)S(1)}, bf16[32,3,2048]{2,1,0:T(4,128)(2,1)S(1)}, u32[]{:S(2)}, u32[]{:S(2)}) collective-permute-start(bf16[32,3,2048]{2,1,0:T(4,128)(2,1)S(1)} %all_to_all.10), channel_id=1, source_target_pairs={{0,1},{1,0},{2,3},{3,2},{4,5},{5,4},{6,7},{7,6},{8,9},{9,8},{10,11... | collective-permute-start | bytes 1179656 | tf_op jit(solution)/shard_map/ppermute | solution.py:24
  71.9 6.9 %copy-start.11 = (f32[12,6]{0,1:T(8,128)S(1)}, f32[12,6]{0,1:T(8,128)}, u32[]{:S(2)}) copy-start(f32[12,6]{0,1:T(8,128)} %param.27) | copy-start | bytes 868
  71.9 2.0 %collective-permute-start.1 = (bf16[32,3,2048]{2,1,0:T(4,128)(2,1)S(1)}, bf16[32,3,2048]{2,1,0:T(4,128)(2,1)S(1)}, u32[]{:S(2)}, u32[]{:S(2)}) collective-permute-start(bf16[32,3,2048]{2,1,0:T(4,128)(2,1)S(1)} %slice.38), channel_id=1, source_target_pairs={{0,1},{1,0},{2,3},{3,2},{4,5},{5,4},{6,7},{7,6},{8,9},{9,8},{10,11... | collective-permute-start | bytes 1179656 | tf_op jit(solution)/shard_map/ppermute | solution.py:24
  75.2 29.2 %all-to-all-start.1 = ((f32[32,3,2048]{2,1,0:T(4,128)}), f32[32,3,2048]{2,1,0:T(4,128)S(1)}, u32[]{:S(2)}, u32[]{:S(2)}) async-start(f32[32,3,2048]{2,1,0:T(4,128)} %convert_add_fusion), calls=%async_computation.1 | async-start | bytes 2097152 | tf_op jit(solution)/shard_map/all_to_all | solution.py:202
where the time goes:
time: 109 us; the launch traced here: 108 us
  matrix products  35.1 us (32%)
  waiting for transfers between devices  28.5 us (26%)
  blocking collectives  22.7 us (21%)
  other arithmetic  10.6 us (10%)
  local copies, waits for them, and re-layouts  6.36 us (6%)
  starting transfers between devices  3.18 us (3%)
  between operations  1.73 us (2%)
    all_to_all x1, waiting for transfers between devices, mix_experts(): lax.all_to_all(pair_sum, 'ep', split_axis=0, concat_axis=0, tiled=True)  24.8 us
    all_to_all x1, blocking collectives, mix_experts(): lax.all_to_all(outgoing.reshape(half_count, per_core, model_width), 'ep',...  22.7 us
    dot_general x2, matrix products, block_step(): jnp.einsum('thc,tpc->thp', q_latent, latent_block, preferred_element_type...  9.26 us
    dot_general x2, matrix products, block_step(): jnp.einsum('thp,tpc->thc', block_probs.astype(jnp.bfloat16), latent_block...  7.5 us
    ppermute x2, waiting for transfers between devices, partner(): return lax.ppermute(value, axis, pairs)  3.68 us
    dot_general x1, matrix products, mix_experts(): jnp.dot(hidden, down_half, preferred_element_type=jnp.float32)  3.47 us
    all_to_all x1, starting transfers between devices, mix_experts(): lax.all_to_all(pair_sum, 'ep', split_axis=0, concat_axis=0, tiled=True)  2.97 us
    dot_general x1, matrix products, attend(): jnp.dot(heads_out, w_out, preferred_element_type=jnp.float32)  2.96 us
  transfers between devices with their start and end apart: 3, of which 3 were waited for; matrix products, arithmetic and copies ran while one was open for 1% of the time, Pallas kernels for 0%

commit v1 on v0

--- a/solution.py
+++ b/solution.py
@@ -1,6 +1,8 @@
 import jax
 import jax.numpy as jnp
 from jax import lax
+from jax.experimental import pallas as pl
+from jax.experimental.pallas import tpu as pltpu
 from jax.sharding import PartitionSpec as P
 
 HEADS = 8
@@ -142,72 +144,245 @@
     return (mixed_attn, new_latent, new_rope_key)
 
 
+MESH = pl.DeviceIdType.MESH
+SUBLANES = 8
+LANES = 128
+
+
 def capacity_of(half_count):
     group_count = half_count // 2 // GROUP_SIZE
     group_most = min(SEQ_DEV, max(3, 2 * ((SEQ_DEV + group_count - 1) // group_count)))
     return (TOP_K * group_most + GROUP_SIZE - 1) // GROUP_SIZE
 
 
-def mix_experts(moe_in, expert_ids, route_weight, expert_gate, expert_up, expert_down):
-    row_count, model_width = moe_in.shape
-    top_count = expert_ids.shape[1]
-    half_count = lax.axis_size("ep")
+def remote(src, dst, send_sem, recv_sem, device):
+    return pltpu.make_async_remote_copy(
+        src_ref=src,
+        dst_ref=dst,
+        send_sem=send_sem,
+        recv_sem=recv_sem,
+        device_id=(device,),
+        device_id_type=MESH,
+    )
+
+
+def greet_all(me, count):
+    barrier = pltpu.get_barrier_semaphore()
+
+    @pl.loop(1, count)
+    def _(step):
+        pl.semaphore_signal(
+            barrier, inc=1, device_id=(lax.rem(me + step, count),), device_id_type=MESH
+        )
+
+    pl.semaphore_wait(barrier, count - 1)
+
+
+def distance(step, count):
+    return lax.rem(count // 2 + step + jnp.where(step >= count // 2, 1, 0), count)
+
+
+def dispatch_kernel(count, out_rows, got, send_sem, recv_sem, pair_send, pair_recv, own_sem):
+    me = lax.axis_index("ep")
+    core = lax.rem(me, 2)
+    sibling = me + 1 - 2 * core
+    own = pltpu.make_async_copy(out_rows.at[me], got.at[core, me], own_sem)
+    own.start()
+    greet_all(me, count)
+
+    @pl.loop(0, count - 1)
+    def _(step):
+        target = lax.rem(me + distance(step, count), count)
+        remote(
+            out_rows.at[target],
+            got.at[lax.rem(target, 2), me],
+            send_sem.at[target],
+            recv_sem.at[me],
+            target,
+        ).start()
+
+    own.wait()
+    remote(
+        got.at[core, me], got.at[core, me], pair_send.at[me], pair_recv.at[me], sibling
+    ).start()
+
+    @pl.loop(0, count - 1)
+    def _(step):
+        source = lax.rem(me + count - distance(step, count), count)
+        place = got.at[core, source]
+        remote(
+            out_rows.at[source], place, send_sem.at[source], recv_sem.at[source], source
+        ).wait_recv()
+        remote(place, place, pair_send.at[source], pair_recv.at[source], sibling).start()
+
+    @pl.loop(0, count - 1)
+    def _(step):
+        target = lax.rem(me + distance(step, count), count)
+        remote(
+            out_rows.at[target],
+            got.at[core, target],
+            send_sem.at[target],
+            recv_sem.at[target],
+            target,
+        ).wait_send()
+
+    @pl.loop(0, count)
+    def _(source):
+        remote(
+            got.at[core, source],
+            got.at[1 - core, source],
+            pair_send.at[source],
+            pair_recv.at[source],
+            sibling,
+        ).wait()
+
+
+def combine_kernel(
+    count, batch, parts, got, from_pair, sums, send_sem, recv_sem, pair_send, pair_recv, own_sem
+):
+    me = lax.axis_index("ep")
+    core = lax.rem(me, 2)
+    sibling = me + 1 - 2 * core
+    batches = count // batch
+    first = me // batch + batches // 2
+    greet_all(me, count)
+
+    def pair_copy(index):
+        span = pl.ds(index * batch, batch)
+        return remote(
+            parts.at[1 - core, span],
+            from_pair.at[span],
+            pair_send.at[index],
+            pair_recv.at[index],
+            sibling,
+        )
+
+    @pl.loop(0, batches)
+    def _(step):
+        pair_copy(lax.rem(first + step, batches)).start()
+
+    @pl.loop(0, batches)
+    def _(step):
+        index = lax.rem(first + step, batches)
+        pair_copy(index).wait_recv()
+        span = pl.ds(index * batch, batch)
+        sums[span] = (
+            parts[core, span].astype(jnp.float32) + from_pair[span].astype(jnp.float32)
+        ).astype(sums.dtype)
+        for place in range(batch):
+            target = index * batch + place
+
+            @pl.when(target != me)
+            def _():
+                remote(
+                    sums.at[target], got.at[me], send_sem.at[target], recv_sem.at[me], target
+                ).start()
+
+    own = pltpu.make_async_copy(sums.at[me], got.at[me], own_sem)
+    own.start()
+
+    @pl.loop(0, batches)
+    def _(index):
+        pair_copy(index).wait_send()
+
+    @pl.loop(1, count)
+    def _(step):
+        other = lax.rem(me + step, count)
+        remote(
+            sums.at[other], got.at[other], send_sem.at[other], recv_sem.at[other], other
+        ).wait()
+
+    own.wait()
+
+
+def dispatch(out_rows):
+    count = out_rows.shape[0]
+    return pl.pallas_call(
+        lambda *refs: dispatch_kernel(count, *refs),
+        out_shape=jax.ShapeDtypeStruct((2,) + out_rows.shape, out_rows.dtype),
+        in_specs=[pl.BlockSpec(memory_space=pltpu.VMEM)],
+        out_specs=pl.BlockSpec(memory_space=pltpu.VMEM),
+        scratch_shapes=[pltpu.SemaphoreType.DMA((count,))] * 4 + [pltpu.SemaphoreType.DMA],
+        compiler_params=pltpu.CompilerParams(collective_id=0, has_side_effects=True),
+        name="dispatch",
+    )(out_rows)
+
+
+def combine(parts):
+    count = parts.shape[1]
+    batch = 4
+    return pl.pallas_call(
+        lambda *refs: combine_kernel(count, batch, *refs),
+        out_shape=jax.ShapeDtypeStruct(parts.shape[1:], parts.dtype),
+        in_specs=[pl.BlockSpec(memory_space=pltpu.VMEM)],
+        out_specs=pl.BlockSpec(memory_space=pltpu.VMEM),
+        scratch_shapes=[pltpu.VMEM(parts.shape[1:], parts.dtype)] * 2
+        + [pltpu.SemaphoreType.DMA((count,))] * 2
+        + [pltpu.SemaphoreType.DMA((count // batch,))] * 2
+        + [pltpu.SemaphoreType.DMA],
+        compiler_params=pltpu.CompilerParams(collective_id=1, has_side_effects=True),
+        name="combine",
+    )(parts)
+
+
+def route_plan(expert_ids, route_weight, half_count):
+    row_count, top_count = expert_ids.shape
+    expert_count = half_count // 2
     slot_count = capacity_of(half_count)
-    per_core = (slot_count + 1) // 2
-    gate_half = expert_gate[0]
-    up_half = expert_up[0]
-    down_half = expert_down[0]
     flat_ids = expert_ids.reshape(-1)
-    one_hot = (flat_ids[:, None] == jnp.arange(half_count // 2, dtype=jnp.int32)[None, :]).astype(
+    one_hot = (flat_ids[:, None] == jnp.arange(expert_count, dtype=jnp.int32)[None, :]).astype(
         jnp.int32
     )
     earlier = jnp.cumsum(one_hot, axis=0) - one_hot
     slot_rank = jnp.sum(earlier * one_hot, axis=1)
-    owner_ids = jnp.arange(half_count, dtype=jnp.int32) // 2
-    parity_ids = jnp.arange(half_count, dtype=jnp.int32) % 2
-    wanted_rank = (
-        2 * jnp.arange(per_core, dtype=jnp.int32)[None, None, :] + parity_ids[None, :, None]
-    )
-    placed = (flat_ids[:, None, None] == owner_ids[None, :, None]) & (
-        slot_rank[:, None, None] == wanted_rank
-    )
-    placed = placed.reshape(row_count * top_count, half_count * per_core).astype(jnp.float32)
-    chosen = jnp.max(placed.reshape(row_count, top_count, half_count * per_core), axis=1).astype(
-        jnp.bfloat16
-    )
+    slot_ids = flat_ids * slot_count + slot_rank
+    placed = slot_ids.reshape(row_count, top_count)[:, :, None] == jnp.arange(
+        expert_count * slot_count, dtype=jnp.int32
+    )
+    chosen = jnp.any(placed, axis=1).astype(jnp.bfloat16)
+    weights = jnp.sum(jnp.where(placed, route_weight[:, :, None], 0.0), axis=1)
+    return chosen, weights
+
+
+def mix_experts(moe_in, plan, expert_gate, expert_up, expert_down):
+    model_width = moe_in.shape[1]
+    half_count = lax.axis_size("ep")
+    expert_count = half_count // 2
+    slot_count = capacity_of(half_count)
+    chosen, weights = plan
+    pieces = model_width // (2 * SUBLANES * LANES) * SUBLANES
     outgoing = jnp.einsum("sx,sd->xd", chosen, moe_in, preferred_element_type=jnp.float32).astype(
         jnp.bfloat16
     )
-    own_rows = lax.all_to_all(
-        outgoing.reshape(half_count, per_core, model_width),
-        "ep",
-        split_axis=0,
-        concat_axis=0,
-        tiled=True,
-    )
-    sibling = partner(own_rows, "ep", 0)
-    slot_rows = jnp.concatenate([own_rows, sibling], axis=1)
-    flat_rows = slot_rows.reshape(-1, model_width)
+    outgoing = (
+        outgoing.reshape(expert_count, slot_count, 2, pieces, LANES)
+        .transpose(0, 2, 1, 3, 4)
+        .reshape(half_count, slot_count, pieces, LANES)
+    )
+    halves = dispatch(outgoing)
+    flat_rows = halves.transpose(1, 2, 0, 3, 4).reshape(half_count * slot_count, model_width)
     hidden = (
-        jax.nn.silu(jnp.dot(flat_rows, gate_half, preferred_element_type=jnp.float32))
-        * jnp.dot(flat_rows, up_half, preferred_element_type=jnp.float32)
+        jax.nn.silu(jnp.dot(flat_rows, expert_gate[0], preferred_element_type=jnp.float32))
+        * jnp.dot(flat_rows, expert_up[0], preferred_element_type=jnp.float32)
     ).astype(jnp.bfloat16)
-    outputs = (
-        jnp.dot(hidden, down_half, preferred_element_type=jnp.float32)
+    parts = (
+        jnp.dot(hidden, expert_down[0], preferred_element_type=jnp.float32)
         .astype(jnp.bfloat16)
-        .reshape(slot_rows.shape)
-    )
-    from_sibling = partner(outputs[:, per_core:], "ep", 0)
-    pair_sum = outputs[:, :per_core].astype(jnp.float32) + from_sibling.astype(jnp.float32)
-    returned = lax.all_to_all(pair_sum, "ep", split_axis=0, concat_axis=0, tiled=True)
-    per_route = jnp.dot(
-        placed,
-        returned.reshape(half_count * per_core, model_width),
+        .reshape(half_count, slot_count, 2, pieces, LANES)
+        .transpose(2, 0, 1, 3, 4)
+    )
+    returned = combine(parts)
+    returned = (
+        returned.reshape(expert_count, 2, slot_count, pieces, LANES)
+        .transpose(0, 2, 1, 3, 4)
+        .reshape(expert_count * slot_count, model_width)
+    )
+    return jnp.dot(
+        weights,
+        returned.astype(jnp.float32),
         precision=lax.Precision.HIGHEST,
         preferred_element_type=jnp.float32,
     )
-    per_route = per_route.reshape(row_count, top_count, model_width)
-    return jnp.sum(route_weight[:, :, None] * per_route, axis=1)
 
 
 def shards(
@@ -248,7 +423,8 @@
         tokens, cache_latent, cache_rope, cache_lengths, *mixer_weights
     )
     moe_in = norm_gain(mixed_attn, moe_gain).astype(jnp.bfloat16)
-    moe_out = mix_experts(moe_in, expert_ids, route_weight, expert_gate, expert_up, expert_down)
+    plan = route_plan(expert_ids, route_weight, lax.axis_size("ep"))
+    moe_out = mix_experts(moe_in, plan, expert_gate, expert_up, expert_down)
     mixed = mixed_attn.astype(jnp.float32) + moe_out
     return (mixed, new_latent, new_rope_key)
 

time: 109 us -> 86.8 us (0.80)
  Pallas kernels: 0 us -> 35 us
  waiting for transfers between devices: 28.5 us -> 0 us
  blocking collectives: 22.7 us -> 0 us
  starting transfers between devices: 3.18 us -> 0 us
  other arithmetic: 10.6 us -> 8.11 us
    pallas_call x0 -> x2, Pallas kernels: none -> 35 us  [the longest x1 18.7 us: dispatch(): pl.pallas_call(lambda *refs: dispatch_kernel(count, *refs), out_shape=jax...]
    all_to_all x1 -> x0, waiting for transfers between devices: 24.8 us -> none  [mix_experts(): lax.all_to_all(pair_sum, 'ep', split_axis=0, concat_axis=0, tiled=True)]
    all_to_all x1 -> x0, blocking collectives: 22.7 us -> none  [mix_experts(): lax.all_to_all(outgoing.reshape(half_count, per_core, model_width), 'ep',...]
    ppermute x2 -> x0, waiting for transfers between devices: 3.68 us -> none  [partner(): return lax.ppermute(value, axis, pairs)]
    all_to_all x1 -> x0, starting transfers between devices: 2.97 us -> none  [mix_experts(): lax.all_to_all(pair_sum, 'ep', split_axis=0, concat_axis=0, tiled=True)]
    add x4 -> x1, other arithmetic: 2.07 us -> 0.01 us  [route_plan(): slot_ids = flat_ids * slot_count + slot_rank]
    dot_general x1, matrix products: 2.27 us -> 0.53 us  [attend(): jnp.dot(normed, w_qdown, preferred_element_type=jnp.float32)]
    unnamed x30 -> x28, local copies, waits for them, and re-layouts: 0.28 us -> 1.82 us
  transfers between devices with their start and end apart: 3 -> 0, of which waited for: 3 -> 0; matrix products, arithmetic and copies ran while one was open for 1% -> 0% of each run, Pallas kernels for 0% -> 0%
where the time goes in v1:
time: 86.8 us; the launch traced here: 85.5 us
  Pallas kernels  35 us (40%)
  matrix products  34.1 us (39%)
  other arithmetic  8.11 us (9%)
  local copies, waits for them, and re-layouts  6.59 us (8%)
  between operations  1.61 us (2%)
    pallas_call x1, Pallas kernels, dispatch(): pl.pallas_call(lambda *refs: dispatch_kernel(count, *refs), out_shape=jax...  18.7 us
    pallas_call x1, Pallas kernels, combine(): pl.pallas_call(lambda *refs: combine_kernel(count, batch, *refs), out_sha...  16.3 us
    dot_general x2, matrix products, block_step(): jnp.einsum('thc,tpc->thp', q_latent, latent_block, preferred_element_type...  9.25 us
    dot_general x2, matrix products, block_step(): jnp.einsum('thp,tpc->thc', block_probs.astype(jnp.bfloat16), latent_block...  7.5 us
    dot_general x1, matrix products, attend(): jnp.dot(heads_out, w_out, preferred_element_type=jnp.float32)  2.96 us
    dot_general x1, matrix products, mix_experts(): jnp.dot(hidden, expert_down[0], preferred_element_type=jnp.float32)  2.54 us
    dot_general x1, matrix products, mix_experts(): jnp.dot(flat_rows, expert_gate[0], preferred_element_type=jnp.float32)  2.22 us
    unnamed x28, local copies, waits for them, and re-layouts  1.82 us

profile of v1, /device:TPU:0, one launch (start us, length us, event | category | flops | bytes accessed | tf_op | source)
XLA Modules:
  0.0 85.5 jit_solution(12635645630612864781)
XLA Ops:
  0.6 0.0 copy-start
  0.6 0.0 copy-start.3
  0.7 0.0 copy-start.6
  0.7 0.0 copy-start.10
  0.7 1.1 %fusion.40 = f32[12]{0:T(128)S(1)} fusion(bf16[12,2048]{1,0:T(8,128)(2,1)} %param.22), kind=kLoop, calls=%fused_computation.53 | loop fusion | flops 73716 | bytes 49200 | tf_op jit(solution)/shard_map/reduce_sum | solution.py:31
  1.8 1.4 %fusion.66 = (s32[]{:T(128)}, f32[12]{0:T(128)S(1)}) fusion(s32[12]{0:T(128)} %param.25), kind=kLoop, calls=%fused_computation.102 | loop fusion | flops 23 | bytes 100 | tf_op jit(solution)/shard_map/reduce_max | solution.py:100
  3.9 0.8 copy.64
  4.7 0.1 eq.28
  4.7 1.2 %fusion.59 = f32[12,64]{1,0:T(8,128)S(1)} fusion(bf16[2048,64]{0,1:T(8,128)(2,1)} %param.34, bf16[12,2048]{1,0:T(8,128)(2,1)} %param.22, f32[2048]{0:T(1024)} %param.28, f32[12]{0:T(128)S(1)} %add_rsqrt_fusion.3), kind=kOutput, calls=%fused_computation.98 | convolution fusion | flops 3244032 | bytes 322608 | tf_op jit(solution)/shard_map/dot_general | solution.py:84
  6.0 0.8 copy.66
  6.8 0.1 subtract_convert_fusion.1
  6.9 0.1 fusion.83
  7.0 0.7 pad_maximum_fusion.1
  7.6 0.0 copy-done
  7.6 1.4 %multiply_reduce_fusion.1 = (f32[12]{0:T(128)S(1)}, f32[12,512]{1,0:T(8,128)S(1)}) fusion(bf16[2048,512]{1,0:T(8,128)(2,1)S(1)} %copy-done, bf16[12,2048]{1,0:T(8,128)(2,1)} %param.22, f32[2048]{0:T(1024)} %param.28, f32[12]{0:T(128)S(1)} %add_rsqrt_fusion.3), kind=kOutput, calls=%fused_computation.73 | convolution fusion | flops 25276404 | bytes 2179168 | tf_op jit(solution)/shard_map/dot_general | solution.py:81
  9.1 0.1 multiply_convert_fusion.2
  9.1 0.7 fusion.82
  9.8 0.0 copy-done.3
  9.8 0.5 multiply_reduce_fusion.2
  10.4 0.1 fusion.48
  10.5 0.1 reduce_window_sum.11
  10.6 0.2 select_reduce_fusion.1
  10.8 0.1 reduce_sum.69
  10.8 0.7 select_reduce_fusion
  11.6 0.7 fusion.47
  12.3 1.8 %fusion.52 = f32[12,1536]{1,0:T(8,128)S(1)} fusion(bf16[512,1536]{1,0:T(8,128)(2,1)} %param.35, f32[12,512]{1,0:T(8,128)S(1)} %get-tuple-element.132, f32[512]{0:T(512)S(1)} %copy-done.11, f32[12]{0:T(128)S(1)} %add_rsqrt_fusion.2), kind=kOutput, calls=%fused_computation.79 | convolution fusion | flops 18892800 | bytes 1673264 | tf_op jit(solution)/shard_map/dot_general | solution.py:74
  14.0 0.1 reshape.171
  14.1 0.1 subtract_convert_fusion
  14.2 0.1 pad_maximum_fusion
  14.3 0.1 fusion.56
  14.4 0.0 copy-done.4
  14.4 0.4 fusion.22
  14.8 0.1 copy.60
  14.9 0.9 %fusion.50 = f32[12,1,8]{2,1,0:T(1,128)S(1)} fusion(bf16[12,8,512]{2,1,0:T(8,128)(2,1)S(1)} %copy.60, bf16[12,512,1]{1,0,2:T(8,128)(2,1)} %fusion.82), kind=kOutput, calls=%fused_computation.77 | convolution fusion | flops 98304 | bytes 110976 | tf_op jit(solution)/shard_map/thc,tc->th/dot_general | solution.py:93
  15.8 19.4 %while.14 = (s32[]{:T(128)}, f32[12,8]{1,0:T(8,128)S(1)}, f32[12,8]{1,0:T(8,128)S(1)}, f32[12,8,512]{2,1,0:T(8,128)S(1)}, s32[]{:T(128)}, /*index=5*/s32[12]{0:T...) while((s32[]{:T(128)}, f32[12,8]{1,0:T(8,128)S(1)}, ...), condition=%wide.region_7.8_spmd, body=%wide.region_4.7_spmd.sunk | while | flops 107453120 | bytes 21184784 | solution.py:127
  15.8 0.7 broadcast_compare_fusion.2
  16.6 4.6 %fusion.100 = f32[12,512,8]{1,2,0:T(8,128)S(1)} fusion(bf16[12,8,512]{2,1,0:T(8,128)(2,1)S(1)} %get-tuple-element.242, bf16[12,1024,512]{2,1,0:T(8,128)(2,1)} %get-tuple-element.241, s32[]{:T(128)S(6)} %select_n.27), kind=kOutput, calls=%fused_computation.2.clone.1 | convolution fusion | flops 50331648 | bytes 6586372 | tf_op jit(solution)/shard_map/while/body/thc,tpc->thp/dot_general | solution.py:108
  21.2 0.3 fusion.101
  21.5 0.2 fusion.102
  21.7 3.7 %fusion.103 = f32[12,8,512]{2,1,0:T(8,128)S(1)} fusion(bf16[12,1024,512]{2,1,0:T(8,128)(2,1)} %get-tuple-element.241, s32[]{:T(128)S(6)} %select_n.27, f32[12,8,512]{2,1,0:T(8,128)S(1)} %get-tuple-element.224, f32[12,8,512]{2,1,0:T(8,128)S(1)} %get-tuple-element.204, f32[12,8]{1,0:T(8,128)S(1)} %get-tuple-element.206, f32[12,8]{1,0:T(8,128)S(1)} %max.4), kind=kOutput, calls=%fused_computation.6.clone.1 | convolution fusion | flops 50528256 | bytes 6882052 | tf_op jit(solution)/shard_map/while/body/thp,tpc->thc/dot_general | solution.py:119
  25.5 0.8 broadcast_compare_fusion.2
  26.3 4.6 %fusion.100 = f32[12,512,8]{1,2,0:T(8,128)S(1)} fusion(bf16[12,8,512]{2,1,0:T(8,128)(2,1)S(1)} %get-tuple-element.242, bf16[12,1024,512]{2,1,0:T(8,128)(2,1)} %get-tuple-element.241, s32[]{:T(128)S(6)} %select_n.27), kind=kOutput, calls=%fused_computation.2.clone.1 | convolution fusion | flops 50331648 | bytes 6586372 | tf_op jit(solution)/shard_map/while/body/thc,tpc->thp/dot_general | solution.py:108
  30.9 0.3 fusion.101
  31.2 0.2 fusion.102
  31.4 3.7 %fusion.103 = f32[12,8,512]{2,1,0:T(8,128)S(1)} fusion(bf16[12,1024,512]{2,1,0:T(8,128)(2,1)} %get-tuple-element.241, s32[]{:T(128)S(6)} %select_n.27, f32[12,8,512]{2,1,0:T(8,128)S(1)} %get-tuple-element.224, f32[12,8,512]{2,1,0:T(8,128)S(1)} %get-tuple-element.204, f32[12,8]{1,0:T(8,128)S(1)} %get-tuple-element.206, f32[12,8]{1,0:T(8,128)S(1)} %max.4), kind=kOutput, calls=%fused_computation.6.clone.1 | convolution fusion | flops 50528256 | bytes 6882052 | tf_op jit(solution)/shard_map/while/body/thp,tpc->thc/dot_general | solution.py:119
  35.2 0.1 divide_convert_fusion
  35.3 1.5 %fusion.24 = bf16[12,8,128]{2,0,1:T(8,128)(2,1)S(1)} fusion(bf16[12,8,512]{2,1,0:T(8,128)(2,1)S(1)} %divide_convert_fusion, bf16[512,1024]{1,0:T(8,128)(2,1)} %param.37), kind=kOutput, calls=%fused_computation.34 | convolution fusion | flops 12595200 | bytes 1171456 | tf_op jit(solution)/shard_map/thc,chv->thv/dot_general | solution.py:132
  36.8 0.0 copy-start.8
  36.9 3.0 %multiply_reduce_fusion = (f32[12]{0:T(128)S(1)}, f32[12,2048]{1,0:T(8,128)S(1)}) fusion(bf16[12,1024]{1,0:T(8,128)(2,1)S(1)} %bitcast.93, bf16[1024,2048]{1,0:T(8,128)(2,1)} %param.38, bf16[12,2048]{1,0:T(8,128)(2,1)S(1)} %copy-done.3), kind=kOutput, calls=%fused_computation.58 | convolution fusion | flops 50479092 | bytes 4366384 | tf_op jit(solution)/shard_map/dot_general | solution.py:142
  39.9 0.3 fusion.21
  40.2 0.1 copy.78
  40.2 0.8 copy.67
  41.0 18.7 %dispatch.1 = bf16[2,32,5,8,128]{4,3,2,1,0:T(8,128)(2,1)} custom-call(bf16[32,5,8,128]{3,2,1,0:T(8,128)(2,1)} %bitcast.91), custom_call_target="tpu_custom_call" | custom-call | tf_op jit(solution)/shard_map/dispatch/pallas_call | solution.py:300
  59.7 1.2 %copy.68 = bf16[32,5,2,8,128]{4,3,2,1,0:T(8,128)(2,1)S(1)} copy(bf16[32,5,2,8,128]{4,3,1,0,2:T(8,128)(2,1)} %bitcast.86) | data formatting | bytes 1310720 | tf_op jit(solution)/shard_map/transpose | solution.py:363
  60.9 0.3 reshape.177
  61.2 2.2 %fusion.31 = f32[160,256]{1,0:T(8,128)} fusion(bf16[160,2048]{1,0:T(8,128)(2,1)S(1)} %reshape.177, bf16[1,2048,256]{2,1,0:T(8,128)(2,1)} %param.39), kind=kOutput, calls=%fused_computation.41 | convolution fusion | flops 167772160 | bytes 1867776 | tf_op jit(solution)/shard_map/dot_general | solution.py:365
  63.4 2.5 %fusion.20 = bf16[20,8,16,128]{3,1,2,0:T(8,128)(2,1)S(1)} fusion(bf16[1,256,2048]{2,1,0:T(8,128)(2,1)} %param.41, bf16[160,2048]{1,0:T(8,128)(2,1)S(1)} %reshape.177, bf16[1,2048,256]{2,1,0:T(8,128)(2,1)} %param.40, f32[160,256]{1,0:T(8,128)} %fusion.31), kind=kOutput, calls=%fused_computation.27 | convolution fusion | flops 336117760 | bytes 3571712 | tf_op jit(solution)/shard_map/dot_general | solution.py:369
  65.9 0.1 copy.79
  66.1 0.0 copy-start.7
  66.1 0.9 %copy.100 = bf16[32,5,2,8,128]{4,3,1,0,2:T(8,128)(2,1)} copy(bf16[32,5,2,8,128]{4,3,2,1,0:T(8,128)(2,1)S(1)} %bitcast.87) | data formatting | bytes 1310720 | tf_op jit(solution)/shard_map/reshape | solution.py:371
  67.0 16.3 %combine.1 = bf16[32,5,8,128]{3,2,1,0:T(8,128)(2,1)} custom-call(bf16[2,32,5,8,128]{4,3,2,1,0:T(8,128)(2,1)} %bitcast.88), custom_call_target="tpu_custom_call" | custom-call | tf_op jit(solution)/shard_map/combine/pallas_call | solution.py:314
  83.4 1.0 %copy.101 = bf16[16,2,5,8,128]{4,3,1,2,0:T(8,128)(2,1)S(1)} copy(bf16[16,2,5,8,128]{4,3,2,1,0:T(8,128)(2,1)} %bitcast.92) | data formatting | bytes 655360 | tf_op jit(solution)/shard_map/reshape | solution.py:376
  84.4 0.1 reshape.180
  84.5 0.9 %convolution_add_fusion.1 = f32[12,2048]{1,0:T(8,128)} fusion(f32[12,2048]{1,0:T(8,128)S(1)} %get-tuple-element.136, f32[12,80]{1,0:T(8,128)S(1)} %copy-done.7, bf16[80,2048]{1,0:T(8,128)(2,1)S(1)} %reshape.180), kind=kOutput, calls=%fused_computation.23 | convolution fusion | flops 23617536 | bytes 528128 | tf_op jit(solution)/shard_map/dot_general | solution.py:380
  (38 shorter events, 0.2 us)
Async XLA Ops:
  0.6 7.0 %copy-start = (bf16[2048,512]{1,0:T(8,128)(2,1)S(1)}, bf16[2048,512]{1,0:T(8,128)(2,1)}, u32[]{:S(2)}) copy-start(bf16[2048,512]{1,0:T(8,128)(2,1)} %param.33) | copy-start | bytes 6291460
  0.6 9.2 %copy-start.3 = (bf16[12,2048]{1,0:T(8,128)(2,1)S(1)}, bf16[12,2048]{1,0:T(8,128)(2,1)}, u32[]{:S(2)}) copy-start(bf16[12,2048]{1,0:T(8,128)(2,1)} %param.22) | copy-start | bytes 147460
  0.7 9.2 %copy-start.6 = (f32[2048]{0:T(1024)S(1)}, f32[2048]{0:T(1024)}, u32[]{:S(2)}) copy-start(f32[2048]{0:T(1024)} %param.28) | copy-start | bytes 24580
  0.7 8.4 %copy-start.10 = (f32[512]{0:T(512)S(1)}, f32[512]{0:T(512)}, u32[]{:S(2)}) copy-start(f32[512]{0:T(512)} %param.30) | copy-start | bytes 6148
  6.8 3.1 %copy-start.2 = (bf16[2048,512]{1,0:T(8,128)(2,1)S(1)}, bf16[2048,512]{1,0:T(8,128)(2,1)}, u32[]{:S(2)}) copy-start(bf16[2048,512]{1,0:T(8,128)(2,1)} %param.32) | copy-start | bytes 6291460
  7.6 4.6 %copy-start.11 = (f32[512]{0:T(512)S(1)}, f32[512]{0:T(512)}, u32[]{:S(2)}) copy-start(f32[512]{0:T(512)} %param.29) | copy-start | bytes 6148
  9.1 6.6 %copy-start.5 = (bf16[12,512]{1,0:T(8,128)(2,1)}, bf16[12,512]{1,0:T(8,128)(2,1)S(1)}, u32[]{:S(2)}) copy-start(bf16[12,512]{1,0:T(8,128)(2,1)S(1)} %multiply_convert_fusion.2) | copy-start | bytes 36868
  9.8 4.6 %copy-start.4 = (bf16[512,1024]{1,0:T(8,128)(2,1)S(1)}, bf16[512,1024]{1,0:T(8,128)(2,1)}, u32[]{:S(2)}) copy-start(bf16[512,1024]{1,0:T(8,128)(2,1)} %param.36) | copy-start | bytes 3145732
  16.6 4.6 %copy-start.1 = (bf16[12,1024,64]{1,2,0:T(8,128)(2,1)S(1)}, bf16[12,1024,64]{1,2,0:T(8,128)(2,1)}, u32[]{:S(2)}) copy-start(bf16[12,1024,64]{1,2,0:T(8,128)(2,1)} %get-tuple-element.243) | copy-start | bytes 4718596 | tf_op jit(solution)/shard_map/while
  26.2 4.6 %copy-start.1 = (bf16[12,1024,64]{1,2,0:T(8,128)(2,1)S(1)}, bf16[12,1024,64]{1,2,0:T(8,128)(2,1)}, u32[]{:S(2)}) copy-start(bf16[12,1024,64]{1,2,0:T(8,128)(2,1)} %get-tuple-element.243) | copy-start | bytes 4718596 | tf_op jit(solution)/shard_map/while
  36.8 3.0 %copy-start.8 = (f32[2048]{0:T(1024)S(1)}, f32[2048]{0:T(1024)}, u32[]{:S(2)}) copy-start(f32[2048]{0:T(1024)} %param.31) | copy-start | bytes 24580
  36.9 3.0 %copy-start.9 = (pred[12,80]{1,0:T(8,128)(4,1)S(1)}, pred[12,80]{1,0:T(8,128)(4,1)}, u32[]{:S(2)}) copy-start(pred[12,80]{1,0:T(8,128)(4,1)} %fusion.47) | copy-start | bytes 2884
  66.1 18.5 %copy-start.7 = (f32[12,80]{1,0:T(8,128)S(1)}, f32[12,80]{1,0:T(8,128)}, u32[]{:S(2)}) copy-start(f32[12,80]{1,0:T(8,128)} %select_reduce_fusion) | copy-start | bytes 11524

commit v2 on v1

--- a/solution.py
+++ b/solution.py
@@ -13,6 +13,7 @@
 GROUP_SIZE = 16
 TOP_K = 6
 BLOCK_POS = 512
+FETCH_POS = 256
 SEQ_DEV = 12
 
 
@@ -47,6 +48,128 @@
         [first_half * cosine - second * sine_part, second * cosine + first_half * sine_part],
         axis=-1,
     )
+
+
+def attend_kernel(
+    scale, lengths, q_latent, q_rope, own, fresh, latent_hbm, rope_hbm, out,
+    latent, rope, scores, probs, sums, latent_sem, rope_sem,
+):
+    rows, places, _ = latent.shape
+    blocks = places // FETCH_POS
+    halves = places // BLOCK_POS
+    per_half = BLOCK_POS // FETCH_POS
+
+    def copies(row, block):
+        span = pl.ds(block * FETCH_POS, FETCH_POS)
+        across = (row, slice(None), span)
+        return (
+            pltpu.make_async_copy(
+                latent_hbm.at[row, span], latent.at[row, span], latent_sem.at[row, block]
+            ),
+            pltpu.make_async_copy(
+                rope_hbm.at[across], rope.at[across], rope_sem.at[row, block]
+            ),
+        )
+
+    @pl.loop(0, rows)
+    def _(row):
+        for block in range(blocks):
+            @pl.when(lengths[row] > block * FETCH_POS)
+            def _():
+                for copy in copies(row, block):
+                    copy.start()
+
+    @pl.loop(0, rows)
+    def _(row):
+        for block in range(blocks):
+            half_start = block // per_half * BLOCK_POS
+
+            @pl.when((lengths[row] <= block * FETCH_POS) & (lengths[row] > half_start))
+            def _():
+                latent[row, pl.ds(block * FETCH_POS, FETCH_POS)] = jnp.zeros(
+                    (FETCH_POS, latent.shape[2]), latent.dtype
+                )
+
+    def score(row, half):
+        span = pl.ds(half * BLOCK_POS, BLOCK_POS)
+        contract = (((1,), (1,)), ((), ()))
+        raw = lax.dot_general(
+            q_latent[row], latent[row, span], contract, preferred_element_type=jnp.float32
+        ) + jnp.dot(
+            q_rope[row], rope[row, :, span], preferred_element_type=jnp.float32
+        )
+        place = half * BLOCK_POS + lax.broadcasted_iota(jnp.int32, raw.shape, 1)
+        scores[row, :, span] = jnp.where(place < lengths[row], raw * scale, -jnp.inf)
+
+    for row in range(rows):
+        for block in range(blocks):
+            @pl.when(lengths[row] > block * FETCH_POS)
+            def _():
+                for copy in copies(row, block):
+                    copy.wait()
+
+        score(row, 0)
+        for half in range(1, halves):
+            @pl.when(lengths[row] > half * BLOCK_POS)
+            def _():
+                score(row, half)
+
+            @pl.when(lengths[row] <= half * BLOCK_POS)
+            def _():
+                scores[row, :, pl.ds(half * BLOCK_POS, BLOCK_POS)] = jnp.full(
+                    (scores.shape[1], BLOCK_POS), -jnp.inf, jnp.float32
+                )
+
+    values = scores[...]
+    own_score = own[...]
+    peak = jnp.maximum(jnp.max(values, axis=2, keepdims=True), own_score)
+    raised = jnp.exp(values - peak)
+    own_prob = jnp.exp(own_score - peak)
+    total = jnp.sum(raised, axis=2, keepdims=True) + own_prob
+    probs[...] = raised.astype(probs.dtype)
+    for row in range(rows):
+        sums[row] = jnp.dot(
+            probs[row, :, :BLOCK_POS], latent[row, :BLOCK_POS], preferred_element_type=jnp.float32
+        )
+    for row in range(rows):
+        for half in range(1, halves):
+            span = pl.ds(half * BLOCK_POS, BLOCK_POS)
+
+            @pl.when(lengths[row] > half * BLOCK_POS)
+            def _():
+                sums[row] += jnp.dot(
+                    probs[row, :, span], latent[row, span], preferred_element_type=jnp.float32
+                )
+
+    out[...] = ((sums[...] + own_prob * fresh[...]) / total).astype(out.dtype)
+
+
+def attend_cached(q_latent, q_rope, own, fresh, lengths, cache_latent, cache_rope, scale):
+    rows, places, width = cache_latent.shape
+    heads = q_latent.shape[1]
+    blocks = places // FETCH_POS
+    vmem = pl.BlockSpec(memory_space=pltpu.VMEM)
+    hbm = pl.BlockSpec(memory_space=pltpu.HBM)
+    read = rows * places * (width + ROPE_DIM)
+    return pl.pallas_call(
+        lambda *refs: attend_kernel(scale, *refs),
+        out_shape=jax.ShapeDtypeStruct((rows, heads, width), jnp.bfloat16),
+        in_specs=[pl.BlockSpec(memory_space=pltpu.SMEM)] + [vmem] * 4 + [hbm] * 2,
+        out_specs=vmem,
+        scratch_shapes=[
+            pltpu.VMEM((rows, places, width), cache_latent.dtype),
+            pltpu.VMEM((rows, ROPE_DIM, places), cache_rope.dtype),
+            pltpu.VMEM((rows, heads, places), jnp.float32),
+            pltpu.VMEM((rows, heads, places), jnp.bfloat16),
+            pltpu.VMEM((rows, heads, width), jnp.float32),
+            pltpu.SemaphoreType.DMA((rows, blocks)),
+            pltpu.SemaphoreType.DMA((rows, blocks)),
+        ],
+        cost_estimate=pl.CostEstimate(
+            flops=4 * heads * read, bytes_accessed=2 * read, transcendentals=rows * heads * places
+        ),
+        name="attend_cached",
+    )(lengths, q_latent, q_rope, own, fresh, cache_latent, jnp.swapaxes(cache_rope, 1, 2))
 
 
 def attend(
@@ -93,41 +216,16 @@
         jnp.einsum("thc,tc->th", q_latent, new_latent, preferred_element_type=jnp.float32)
         + jnp.einsum("thr,tr->th", q_rope, new_rope_key, preferred_element_type=jnp.float32)
     ) * score_scale
-    run_sum = jnp.broadcast_to(
-        new_latent.astype(jnp.float32)[:, None, :], (row_count, HEADS, KV_RANK)
-    )
-    run_total = jnp.ones((row_count, HEADS), jnp.float32)
-    block_total = (jnp.max(cache_lengths) + BLOCK_POS - 1) // BLOCK_POS
-
-    def block_step(block_index, carry):
-        run_peak, run_total, run_sum = carry
-        block_start = block_index * BLOCK_POS
-        latent_block = lax.dynamic_slice_in_dim(cache_latent, block_start, BLOCK_POS, 1)
-        rope_block = lax.dynamic_slice_in_dim(cache_rope, block_start, BLOCK_POS, 1)
-        scores = (
-            jnp.einsum("thc,tpc->thp", q_latent, latent_block, preferred_element_type=jnp.float32)
-            + jnp.einsum("thr,tpr->thp", q_rope, rope_block, preferred_element_type=jnp.float32)
-        ) * score_scale
-        valid_mask = (block_start + jnp.arange(BLOCK_POS, dtype=jnp.int32))[
-            None, None, :
-        ] < cache_lengths[:, None, None]
-        scores = jnp.where(valid_mask, scores, -jnp.inf)
-        new_peak = jnp.maximum(run_peak, jnp.max(scores, axis=2))
-        shrink = jnp.exp(run_peak - new_peak)
-        block_probs = jnp.exp(scores - new_peak[:, :, None])
-        run_total = run_total * shrink + jnp.sum(block_probs, axis=2)
-        run_sum = run_sum * shrink[:, :, None] + jnp.einsum(
-            "thp,tpc->thc",
-            block_probs.astype(jnp.bfloat16),
-            latent_block,
-            preferred_element_type=jnp.float32,
-        )
-        return (new_peak, run_total, run_sum)
-
-    run_peak, run_total, run_sum = lax.fori_loop(
-        0, block_total, block_step, (own_score, run_total, run_sum)
-    )
-    o_latent = (run_sum / run_total[:, :, None]).astype(jnp.bfloat16)
+    o_latent = attend_cached(
+        q_latent,
+        q_rope,
+        own_score[:, :, None],
+        new_latent.astype(jnp.float32)[:, None, :],
+        cache_lengths,
+        cache_latent,
+        cache_rope,
+        score_scale,
+    )
     heads_out = (
         jnp.einsum(
             "thc,chv->thv",

time: 86.8 us -> 77.2 us (0.89); the launches traced: 85.5 us -> 77.2 us
  matrix products: 34.1 us -> 16 us
  Pallas kernels: 35 us -> 47.3 us
  other arithmetic: 8.11 us -> 4.76 us
  local copies, waits for them, and re-layouts: 6.59 us -> 8.13 us
    dot_general x6 -> x0, matrix products: 17.4 us -> none  [the longest x2 9.25 us: block_step(): jnp.einsum('thc,tpc->thp', q_latent, latent_block, preferred_element_type...]
    pallas_call x0 -> x1, Pallas kernels: none -> 8.66 us  [attend_cached(): pl.pallas_call(lambda *refs: attend_kernel(scale, *refs), out_shape=jax.S...]
    pallas_call x1, Pallas kernels: 18.7 us -> 22.5 us  [dispatch(): pl.pallas_call(lambda *refs: dispatch_kernel(count, *refs), out_shape=jax...]
    lt x2 -> x0, other arithmetic: 1.48 us -> none  [block_step(): (block_start + jnp.arange(BLOCK_POS, dtype=jnp.int32))[None, None, :]]
    reduce_max x1 -> x0, other arithmetic: 1.38 us -> none  [attend(): block_total = (jnp.max(cache_lengths) + BLOCK_POS - 1) // BLOCK_POS]
    broadcast_in_dim x2, local copies, waits for them, and re-layouts: 0.03 us -> 1.39 us  [the longest x1 0.77 us: attend(): own_score[:, :, None]]
    unnamed x28 -> x32, local copies, waits for them, and re-layouts: 1.82 us -> 1.84 us
where the time goes in v2:
time: 77.2 us
  Pallas kernels  47.3 us (61%)
  matrix products  16 us (21%)
  local copies, waits for them, and re-layouts  8.13 us (11%)
  other arithmetic  4.76 us (6%)
  between operations  0.93 us (1%)
    pallas_call x1, Pallas kernels, dispatch(): pl.pallas_call(lambda *refs: dispatch_kernel(count, *refs), out_shape=jax...  22.5 us
    pallas_call x1, Pallas kernels, combine(): pl.pallas_call(lambda *refs: combine_kernel(count, batch, *refs), out_sha...  16.2 us
    pallas_call x1, Pallas kernels, attend_cached(): pl.pallas_call(lambda *refs: attend_kernel(scale, *refs), out_shape=jax.S...  8.66 us
    dot_general x1, matrix products, attend(): jnp.dot(heads_out, w_out, preferred_element_type=jnp.float32)  2.96 us
    dot_general x1, matrix products, mix_experts(): jnp.dot(hidden, expert_down[0], preferred_element_type=jnp.float32)  2.54 us
    dot_general x1, matrix products, mix_experts(): jnp.dot(flat_rows, expert_gate[0], preferred_element_type=jnp.float32)  2.22 us
    unnamed x32, local copies, waits for them, and re-layouts  1.84 us
    dot_general x1, matrix products, attend(): jnp.dot(q_low, w_qup, preferred_element_type=jnp.float32)  1.76 us

profile of v2, /device:TPU:0, one launch (start us, length us, event | category | flops | bytes accessed | tf_op | source)
XLA Modules:
  0.0 77.2 jit_solution(8815042955103369911)
XLA Ops:
  0.6 0.0 copy-start
  0.6 0.0 copy-start.2
  0.7 0.0 copy-start.7
  0.7 0.0 copy-start.11
  0.7 0.8 %convert_element_type.60 = f32[12]{0:T(128)S(1)} convert(s32[12]{0:T(128)} %refs_0_.1) | non-fusion elementwise | flops 12 | bytes 96 | tf_op jit(solution)/shard_map/convert_element_type | solution.py:38
  1.5 1.0 %fusion.22 = f32[12]{0:T(128)S(1)} fusion(bf16[12,2048]{1,0:T(8,128)(2,1)} %param.20), kind=kLoop, calls=%fused_computation.31 | loop fusion | flops 73716 | bytes 49200 | tf_op jit(solution)/shard_map/reduce_sum | solution.py:32
  2.5 0.8 %copy.54 = s32[12,6]{1,0:T(8,128)S(1)} copy(s32[12,6]{0,1:T(8,128)} %param.24) | data formatting | bytes 576 | tf_op args[4]
  3.3 0.1 eq.28
  3.4 1.2 %fusion.43 = f32[12,64]{1,0:T(8,128)S(1)} fusion(bf16[2048,64]{0,1:T(8,128)(2,1)} %param.32, bf16[12,2048]{1,0:T(8,128)(2,1)} %param.20, f32[2048]{0:T(1024)} %param.26, f32[12]{0:T(128)S(1)} %add_rsqrt_fusion.3), kind=kOutput, calls=%fused_computation.78 | convolution fusion | flops 3244032 | bytes 322608 | tf_op jit(solution)/shard_map/dot_general | solution.py:207
  4.6 0.8 %copy.56 = f32[12,6]{1,0:T(8,128)S(1)} copy(f32[12,6]{0,1:T(8,128)} %param.25) | data formatting | bytes 576 | tf_op args[5]
  5.4 0.1 subtract_convert_fusion.1
  5.5 0.1 fusion.63
  5.6 0.7 pad_maximum_fusion.1
  6.3 0.0 copy-done
  6.3 1.4 %multiply_reduce_fusion.1 = (f32[12]{0:T(128)S(1)}, f32[12,512]{1,0:T(8,128)S(1)}) fusion(bf16[2048,512]{1,0:T(8,128)(2,1)S(1)} %copy-done, bf16[12,2048]{1,0:T(8,128)(2,1)} %param.20, f32[2048]{0:T(1024)} %param.26, f32[12]{0:T(128)S(1)} %add_rsqrt_fusion.3), kind=kOutput, calls=%fused_computation.52 | convolution fusion | flops 25276404 | bytes 2179168 | tf_op jit(solution)/shard_map/dot_general | solution.py:204
  7.7 0.0 copy-done.11
  7.7 0.1 multiply_convert_fusion.2
  7.7 0.1 fusion.62
  7.8 0.6 reshape.144.refs_4_
  8.4 0.0 copy-done.2
  8.4 0.0 copy-done.7
  8.4 0.0 copy-done.1
  8.5 0.5 multiply_reduce_fusion.2
  9.0 0.1 fusion.31
  9.1 0.1 reduce_window_sum.11
  9.2 0.2 select_reduce_fusion.1
  9.4 0.1 reduce_sum.60
  9.5 0.7 select_reduce_fusion
  10.2 0.7 fusion.30
  10.8 0.0 copy-done.12
  10.9 1.8 %fusion.35 = f32[12,1536]{1,0:T(8,128)S(1)} fusion(bf16[512,1536]{1,0:T(8,128)(2,1)} %param.33, f32[12,512]{1,0:T(8,128)S(1)} %get-tuple-element.10, f32[512]{0:T(512)S(1)} %copy-done.12, f32[12]{0:T(128)S(1)} %add_rsqrt_fusion.2), kind=kOutput, calls=%fused_computation.58 | convolution fusion | flops 18892800 | bytes 1673264 | tf_op jit(solution)/shard_map/dot_general | solution.py:197
  12.6 0.0 copy-done.6
  12.6 0.1 reshape.134
  12.7 0.1 subtract_convert_fusion
  12.8 0.1 pad_maximum_fusion.refs_2_
  12.9 0.1 fusion.38
  13.0 0.1 copy.64
  13.1 0.0 copy-done.3
  13.1 0.4 fusion.8
  13.5 0.1 copy.93
  13.6 0.0 copy-start.4
  13.6 0.1 fusion.33
  13.7 0.1 copy.62
  13.8 0.8 copy.50.refs_3_
  14.6 0.0 copy-done.5
  14.6 0.0 copy-done.4
  14.6 8.7 %attend_cached.1 = bf16[12,8,512]{2,1,0:T(8,128)(2,1)} custom-call(s32[12]{0:T(128)} %refs_0_.1, bf16[12,8,512]{2,1,0:T(8,128)(2,1)} %bitcast.93, bf16[12,8,64]{2,1,0:T(8,128)(2,1)} %copy-done.5, f32[12,8,1]{2,1,0:T(8,128)} %copy.50.refs_3_, f32[12,1,512]{2,1,0:T(1,128)} %reshape.144.refs_4_, bf16[12,1024,512]{2,1,0:T(8,128)(2,1)} %refs_5_.1, ...), custom_call_target="tpu_custom_call" | custom-call | flops 226492416 | bytes 14155776 | tf_op jit(solution)/shard_map/attend_cached/pallas_call | solution.py:154
  23.3 1.6 %fusion.5 = bf16[12,8,128]{2,0,1:T(8,128)(2,1)S(1)} fusion(bf16[12,8,512]{2,1,0:T(8,128)(2,1)} %attend_cached.1, bf16[512,1024]{1,0:T(8,128)(2,1)} %param.35), kind=kOutput, calls=%fused_computation.11 | convolution fusion | flops 12595200 | bytes 1171456 | tf_op jit(solution)/shard_map/thc,chv->thv/dot_general | solution.py:230
  24.9 0.0 copy-start.9
  24.9 3.0 %multiply_reduce_fusion = (f32[12]{0:T(128)S(1)}, f32[12,2048]{1,0:T(8,128)S(1)}) fusion(bf16[12,1024]{1,0:T(8,128)(2,1)S(1)} %bitcast.94, bf16[1024,2048]{1,0:T(8,128)(2,1)} %param.36, bf16[12,2048]{1,0:T(8,128)(2,1)S(1)} %copy-done.2), kind=kOutput, calls=%fused_computation.36 | convolution fusion | flops 50479092 | bytes 4366384 | tf_op jit(solution)/shard_map/dot_general | solution.py:240
  27.9 0.3 fusion.3
  28.2 0.1 copy.68
  28.3 0.8 %copy.57 = bf16[16,5,2,8,128]{4,3,1,2,0:T(8,128)(2,1)} copy(bf16[16,5,2,8,128]{4,3,2,1,0:T(8,128)(2,1)S(1)} %bitcast.88) | data formatting | bytes 655360 | tf_op jit(solution)/shard_map/reshape | solution.py:456
  29.1 22.5 %dispatch.1 = bf16[2,32,5,8,128]{4,3,2,1,0:T(8,128)(2,1)} custom-call(bf16[32,5,8,128]{3,2,1,0:T(8,128)(2,1)} %bitcast.90), custom_call_target="tpu_custom_call" | custom-call | tf_op jit(solution)/shard_map/dispatch/pallas_call | solution.py:398
  51.5 1.2 %copy.58 = bf16[32,5,2,8,128]{4,3,2,1,0:T(8,128)(2,1)S(1)} copy(bf16[32,5,2,8,128]{4,3,1,0,2:T(8,128)(2,1)} %bitcast.84) | data formatting | bytes 1310720 | tf_op jit(solution)/shard_map/transpose | solution.py:461
  52.7 0.3 reshape.140
  53.0 2.2 %fusion.13 = f32[160,256]{1,0:T(8,128)} fusion(bf16[160,2048]{1,0:T(8,128)(2,1)S(1)} %reshape.140, bf16[1,2048,256]{2,1,0:T(8,128)(2,1)} %param.37), kind=kOutput, calls=%fused_computation.19 | convolution fusion | flops 167772160 | bytes 1867776 | tf_op jit(solution)/shard_map/dot_general | solution.py:463
  55.2 2.5 %fusion.2 = bf16[20,8,16,128]{3,1,2,0:T(8,128)(2,1)S(1)} fusion(bf16[1,256,2048]{2,1,0:T(8,128)(2,1)} %param.39, bf16[160,2048]{1,0:T(8,128)(2,1)S(1)} %reshape.140, bf16[1,2048,256]{2,1,0:T(8,128)(2,1)} %param.38, f32[160,256]{1,0:T(8,128)} %fusion.13), kind=kOutput, calls=%fused_computation.6 | convolution fusion | flops 336117760 | bytes 3571712 | tf_op jit(solution)/shard_map/dot_general | solution.py:467
  57.8 0.1 copy.69
  57.9 0.9 %copy.91 = bf16[32,5,2,8,128]{4,3,1,0,2:T(8,128)(2,1)} copy(bf16[32,5,2,8,128]{4,3,2,1,0:T(8,128)(2,1)S(1)} %bitcast.85) | data formatting | bytes 1310720 | tf_op jit(solution)/shard_map/reshape | solution.py:469
  58.9 16.2 %combine.1 = bf16[32,5,8,128]{3,2,1,0:T(8,128)(2,1)} custom-call(bf16[2,32,5,8,128]{4,3,2,1,0:T(8,128)(2,1)} %bitcast.86), custom_call_target="tpu_custom_call" | custom-call | tf_op jit(solution)/shard_map/combine/pallas_call | solution.py:412
  75.1 1.0 %copy.92 = bf16[16,2,5,8,128]{4,3,1,2,0:T(8,128)(2,1)S(1)} copy(bf16[16,2,5,8,128]{4,3,2,1,0:T(8,128)(2,1)} %bitcast.91) | data formatting | bytes 655360 | tf_op jit(solution)/shard_map/reshape | solution.py:474
  76.1 0.1 reshape.143
  76.2 0.9 %convolution_add_fusion = f32[12,2048]{1,0:T(8,128)} fusion(f32[12,2048]{1,0:T(8,128)S(1)} %get-tuple-element.14, f32[12,80]{1,0:T(8,128)S(1)} %copy-done.8, bf16[80,2048]{1,0:T(8,128)(2,1)S(1)} %reshape.143), kind=kOutput, calls=%fused_computation.2 | convolution fusion | flops 23617536 | bytes 528128 | tf_op jit(solution)/shard_map/dot_general | solution.py:478
  (21 shorter events, 0.1 us)
Async XLA Ops:
  0.6 5.6 %copy-start = (bf16[2048,512]{1,0:T(8,128)(2,1)S(1)}, bf16[2048,512]{1,0:T(8,128)(2,1)}, u32[]{:S(2)}) copy-start(bf16[2048,512]{1,0:T(8,128)(2,1)} %param.31) | copy-start | bytes 6291460
  0.6 7.8 %copy-start.2 = (bf16[12,2048]{1,0:T(8,128)(2,1)S(1)}, bf16[12,2048]{1,0:T(8,128)(2,1)}, u32[]{:S(2)}) copy-start(bf16[12,2048]{1,0:T(8,128)(2,1)} %param.20) | copy-start | bytes 147460
  0.7 7.8 %copy-start.7 = (f32[2048]{0:T(1024)S(1)}, f32[2048]{0:T(1024)}, u32[]{:S(2)}) copy-start(f32[2048]{0:T(1024)} %param.26) | copy-start | bytes 24580
  0.7 7.0 %copy-start.11 = (f32[512]{0:T(512)S(1)}, f32[512]{0:T(512)}, u32[]{:S(2)}) copy-start(f32[512]{0:T(512)} %param.28) | copy-start | bytes 6148
  5.4 3.1 %copy-start.1 = (bf16[2048,512]{1,0:T(8,128)(2,1)S(1)}, bf16[2048,512]{1,0:T(8,128)(2,1)}, u32[]{:S(2)}) copy-start(bf16[2048,512]{1,0:T(8,128)(2,1)} %param.30) | copy-start | bytes 6291460
  6.3 4.6 %copy-start.12 = (f32[512]{0:T(512)S(1)}, f32[512]{0:T(512)}, u32[]{:S(2)}) copy-start(f32[512]{0:T(512)} %param.27) | copy-start | bytes 6148
  7.7 4.9 %copy-start.6 = (bf16[12,512]{1,0:T(8,128)(2,1)}, bf16[12,512]{1,0:T(8,128)(2,1)S(1)}, u32[]{:S(2)}) copy-start(bf16[12,512]{1,0:T(8,128)(2,1)S(1)} %multiply_convert_fusion.2) | copy-start | bytes 36868
  8.5 4.7 %copy-start.3 = (bf16[512,1024]{1,0:T(8,128)(2,1)S(1)}, bf16[512,1024]{1,0:T(8,128)(2,1)}, u32[]{:S(2)}) copy-start(bf16[512,1024]{1,0:T(8,128)(2,1)} %param.34) | copy-start | bytes 3145732
  12.9 1.7 %copy-start.5 = (bf16[12,8,64]{2,1,0:T(8,128)(2,1)}, bf16[12,8,64]{2,1,0:T(8,128)(2,1)S(1)}, u32[]{:S(2)}) copy-start(bf16[12,8,64]{2,1,0:T(8,128)(2,1)S(1)} %pad_maximum_fusion.refs_2_) | copy-start | bytes 36868
  13.6 1.0 %copy-start.4 = (bf16[8,12,512]{2,0,1:T(8,128)(2,1)}, bf16[8,12,512]{2,0,1:T(8,128)(2,1)S(1)}, u32[]{:S(2)}) copy-start(bf16[8,12,512]{2,0,1:T(8,128)(2,1)S(1)} %copy.93) | copy-start | bytes 294916
  24.9 3.0 %copy-start.9 = (f32[2048]{0:T(1024)S(1)}, f32[2048]{0:T(1024)}, u32[]{:S(2)}) copy-start(f32[2048]{0:T(1024)} %param.29) | copy-start | bytes 24580
  24.9 3.0 %copy-start.10 = (pred[12,80]{1,0:T(8,128)(4,1)S(1)}, pred[12,80]{1,0:T(8,128)(4,1)}, u32[]{:S(2)}) copy-start(pred[12,80]{1,0:T(8,128)(4,1)} %fusion.30) | copy-start | bytes 2884
  57.9 18.3 %copy-start.8 = (f32[12,80]{1,0:T(8,128)S(1)}, f32[12,80]{1,0:T(8,128)}, u32[]{:S(2)}) copy-start(f32[12,80]{1,0:T(8,128)} %select_reduce_fusion) | copy-start | bytes 11524
